TPU v7x, 32 devices: a whole 2x2x4 slice. The times are simulated.
32 devices in a mesh: grp: 2 (over x), sp: 4 (over z), tp: 4 (over y, core).
Axes of the slice: x: 2, y: 2, z: 4, core: 2. Of those that a mesh axis runs over, the one named last changes fastest.
Arguments:
- tokens: bfloat16 [1792, 4096], P(('grp', 'sp'), 'tp'), parts along dimension 0, may hold values from -130 to 130
- rms_gain: float32 [2, 4096], replicated, may hold values from 0.1 to 1.9
- w_value: bfloat16 [2, 4096, 2048], P(None, 'sp', 'tp'), may hold values from -0.09375 to 0.09375
- w_gate: bfloat16 [2, 4096, 2048], P(None, 'sp', 'tp'), may hold values from -0.09375 to 0.09375
- taps: float32 [2, 31, 2048], P(None, None, 'tp'), may hold values from -8 to 8
- ln_gain: float32 [2, 2048], P(None, 'tp'), may hold values from 0.1 to 1.9
- ln_bias: float32 [2, 2048], P(None, 'tp'), may hold values from -3 to 3
- w_out: bfloat16 [2, 2048, 4096], P(None, 'sp', 'tp'), may hold values from -0.125 to 0.125
Outputs:
- result: bfloat16 [1792, 4096], P(('grp', 'sp'), 'tp'), parts along dimension 0
There are 2 independent parts, one for each index of `grp`. A program takes and returns all parts, laid end to end along the dimension named above; an argument that names none is the same for every part. Nothing has to cross between parts.
All inputs are finite; a program needn't handle non-finite values.
Results may differ from a plain program's by a relative error of at most 0.009.
Values may be sent and summed in bfloat16 or wider, within the bound.
A program may use at most 64 MiB of HBM per device.

v0:
```python
import jax
import jax.numpy as jnp
from jax import lax
from jax.sharding import PartitionSpec as P

CH = 2048


def passed_along(block, axis, distance):
    devices = range(lax.axis_size(axis))
    route = [(i - distance, i) for i in devices if i - distance in devices]
    return lax.ppermute(block, axis, route)


def project_in(weight, columns):
    return lax.dot_general(
        weight, columns, (((0,), (1,)), ((), ())), preferred_element_type=jnp.float32
    )


def project_out(rows, weight):
    return lax.dot_general(
        rows, weight, (((0,), (0,)), ((), ())), preferred_element_type=jnp.float32
    )


def norm_rows(wide, gain):
    return (wide * lax.rsqrt(jnp.mean(wide * wide, axis=1, keepdims=True) + 1e-06) * gain).astype(
        jnp.bfloat16
    )


def shards(tokens, rms_gain, w_value, w_gate, taps, ln_gain, ln_bias, w_out):
    layers = w_value.shape[0]
    tok_rows = tokens.shape[0]
    chans = w_value.shape[2]
    reach = taps.shape[1]
    current = tokens
    for layer in range(layers):
        gain = rms_gain[layer]
        whole_rows = lax.all_gather(current, "tp", axis=1, tiled=True)
        normed = norm_rows(whole_rows.astype(jnp.float32), gain)
        value_t = project_in(lax.all_gather(w_value[layer], "sp", axis=0, tiled=True), normed)
        gate_t = project_in(lax.all_gather(w_gate[layer], "sp", axis=0, tiled=True), normed)
        glu_t = (value_t * jax.nn.sigmoid(gate_t)).astype(jnp.bfloat16)
        earlier = passed_along(glu_t[:, tok_rows - (reach - 1) :], "sp", 1)
        extended = jnp.concatenate([earlier, glu_t], axis=1).astype(jnp.float32)
        layer_taps = taps[layer]
        conv = jnp.zeros((chans, tok_rows), jnp.float32)
        for k in range(reach):
            conv = conv + layer_taps[k][:, None] * extended[:, k : k + tok_rows]
        total, total_sq = lax.psum((jnp.sum(conv, axis=0), jnp.sum(conv * conv, axis=0)), "tp")
        mean = total / CH
        var = total_sq / CH - mean * mean
        shaped = (conv - mean[None, :]) * lax.rsqrt(var + 1e-05)[None, :] * ln_gain[layer][
            :, None
        ] + ln_bias[layer][:, None]
        act_t = jax.nn.silu(shaped).astype(jnp.bfloat16)
        act_all = lax.all_gather(act_t, "tp", axis=0, tiled=True)
        branch = project_out(act_all, lax.all_gather(w_out[layer], "sp", axis=0, tiled=True))
        current = (current.astype(jnp.float32) + branch).astype(jnp.bfloat16)
    return current


def solution(mesh):
    return jax.shard_map(
        shards,
        mesh=mesh,
        in_specs=(
            P(("grp", "sp"), "tp"),
            P(),
            P(None, "sp", "tp"),
            P(None, "sp", "tp"),
            P(None, None, "tp"),
            P(None, "tp"),
            P(None, "tp"),
            P(None, "sp", "tp"),
        ),
        out_specs=P(("grp", "sp"), "tp"),
        check_vma=False,
    )
```

profile of v0, /device:TPU:0, one launch (start us, length us, event | category | flops | bytes accessed | tf_op | source)
XLA Modules:
  0.0 555.3 jit_solution(11916564640636365866)
XLA Ops:
  7.3 3.0 fusion.142
  11.9 3.0 fusion.140
  15.2 17.5 %all-gather.15.cloned.1.call-done = bf16[224,4096]{1,0:T(8,128)(2,1)} async-done(((bf16[224,1024]{1,0:T(8,128)(2,1)}), bf16[224,4096]{1,0:T(8,128)(2,1)}) %all-gather.15.cloned.1.call-update) | async-done | bytes 1835024 | tf_op jit(solution)/shard_map/all_gather | solution.py:41
  32.8 1.9 fusion.12
  34.7 80.4 %all-gather.21.cloned.1.call-done = bf16[1,4096,512]{2,1,0:T(8,128)(2,1)} async-done(((bf16[1,1024,512]{2,1,0:T(8,128)(2,1)}), bf16[1,4096,512]{2,1,0:T(8,128)(2,1)}) %all-gather.21.cloned.1.call-update) | async-done | bytes 4194320 | tf_op jit(solution)/shard_map/all_gather | solution.py:44
  115.1 4.1 fusion.57
  119.2 76.7 %all-gather.19.cloned.1.call-done = bf16[1,4096,512]{2,1,0:T(8,128)(2,1)} async-done(((bf16[1,1024,512]{2,1,0:T(8,128)(2,1)}), bf16[1,4096,512]{2,1,0:T(8,128)(2,1)}) %all-gather.19.cloned.1.call-update) | async-done | bytes 4194320 | tf_op jit(solution)/shard_map/all_gather | solution.py:43
  195.9 3.3 fusion.66
  202.2 2.4 fusion.137
  204.6 6.3 %all-reduce.1 = (f32[224]{0:T(256)S(1)}, f32[224]{0:T(256)S(1)}) all-reduce(f32[224]{0:T(256)S(1)} %get-tuple-element.8, f32[224]{0:T(256)S(1)} %get-tuple-element.7), channel_id=1, replica_groups=mesh['grp'=2,'sp'=4,'tp'=4] {'tp'}, use_global_device_ids=true, to_apply=%region_4.0 | all-reduce | flops 448 | bytes 3584 | tf_op jit(solution)/shard_map/psum | solution.py:52
  211.2 9.1 %all_gather.33 = bf16[2048,224]{0,1:T(8,128)(2,1)S(1)} all-gather(bf16[512,224]{0,1:T(8,128)(2,1)S(1)} %multiply_convert_fusion.1), channel_id=1, replica_groups=mesh['grp'=2,'sp'=4,'tp'=4] {'tp'}, dimensions={0}, use_global_device_ids=true | all-gather | bytes 1146880 | tf_op jit(solution)/shard_map/all_gather | solution.py:59
  220.3 56.3 %all-gather.23.cloned.1.call-done = bf16[1,2048,1024]{2,1,0:T(8,128)(2,1)} async-done(((bf16[1,512,1024]{2,1,0:T(8,128)(2,1)}), bf16[1,2048,1024]{2,1,0:T(8,128)(2,1)}) %all-gather.23.cloned.1.call-update) | async-done | bytes 4194320 | tf_op jit(solution)/shard_map/all_gather | solution.py:60
  276.6 4.1 fusion.27
  282.8 17.7 %all-gather.17.cloned.1.call-done = bf16[224,4096]{1,0:T(8,128)(2,1)} async-done(((bf16[224,1024]{1,0:T(8,128)(2,1)}), bf16[224,4096]{1,0:T(8,128)(2,1)}) %all-gather.17.cloned.1.call-update) | async-done | bytes 1835024 | tf_op jit(solution)/shard_map/all_gather | solution.py:41
  300.5 1.9 fusion.15
  302.4 80.2 %all-gather.27.cloned.1.call-done = bf16[1,4096,512]{2,1,0:T(8,128)(2,1)} async-done(((bf16[1,1024,512]{2,1,0:T(8,128)(2,1)}), bf16[1,4096,512]{2,1,0:T(8,128)(2,1)}) %all-gather.27.cloned.1.call-update) | async-done | bytes 4194320 | tf_op jit(solution)/shard_map/all_gather | solution.py:44
  382.7 4.1 fusion.51
  386.8 76.7 %all-gather.25.cloned.1.call-done = bf16[1,4096,512]{2,1,0:T(8,128)(2,1)} async-done(((bf16[1,1024,512]{2,1,0:T(8,128)(2,1)}), bf16[1,4096,512]{2,1,0:T(8,128)(2,1)}) %all-gather.25.cloned.1.call-update) | async-done | bytes 4194320 | tf_op jit(solution)/shard_map/all_gather | solution.py:43
  463.5 3.3 fusion.69
  469.8 2.4 fusion.136
  472.2 6.3 %all-reduce = (f32[224]{0:T(256)S(1)}, f32[224]{0:T(256)S(1)}) all-reduce(f32[224]{0:T(256)S(1)} %get-tuple-element.6, f32[224]{0:T(256)S(1)} %get-tuple-element.5), channel_id=1, replica_groups=mesh['grp'=2,'sp'=4,'tp'=4] {'tp'}, use_global_device_ids=true, to_apply=%region_9.10 | all-reduce | flops 448 | bytes 3584 | tf_op jit(solution)/shard_map/psum | solution.py:52
  478.8 9.1 %all_gather.38 = bf16[2048,224]{0,1:T(8,128)(2,1)S(1)} all-gather(bf16[512,224]{0,1:T(8,128)(2,1)S(1)} %multiply_convert_fusion), channel_id=1, replica_groups=mesh['grp'=2,'sp'=4,'tp'=4] {'tp'}, dimensions={0}, use_global_device_ids=true | all-gather | bytes 1146880 | tf_op jit(solution)/shard_map/all_gather | solution.py:59
  487.9 56.5 %all-gather.29.cloned.1.call-done = bf16[1,2048,1024]{2,1,0:T(8,128)(2,1)} async-done(((bf16[1,512,1024]{2,1,0:T(8,128)(2,1)}), bf16[1,2048,1024]{2,1,0:T(8,128)(2,1)}) %all-gather.29.cloned.1.call-update) | async-done | bytes 4194320 | tf_op jit(solution)/shard_map/all_gather | solution.py:60
  544.3 4.1 fusion.24
  (56 shorter events, 11.0 us)
Async XLA Ops:
  6.5 3.9 copy-start
  6.5 26.2 %all-gather.15.cloned.1.call-start = ((), (), s32[]{:S(2)}) async-start(), calls=%async_computation | async-start | bytes 2293760 | tf_op jit(solution)/shard_map/all_gather | solution.py:41
  7.3 107.8 %all-gather.21.cloned.1.call-start = ((), (), s32[]{:S(2)}) async-start(), calls=%async_computation.3 | async-start | bytes 5242880 | tf_op jit(solution)/shard_map/all_gather | solution.py:44
  10.3 185.6 %all-gather.19.cloned.1.call-start = ((), (), s32[]{:S(2)}) async-start(), calls=%async_computation.2 | async-start | bytes 5242880 | tf_op jit(solution)/shard_map/all_gather | solution.py:43
  11.9 3.2 copy-start.7
  11.9 3.2 copy-start.5
  11.9 3.3 copy-start.6
  11.9 264.7 %all-gather.23.cloned.1.call-start = ((), (), s32[]{:S(2)}) async-start(), calls=%async_computation.4 | async-start | bytes 5242880 | tf_op jit(solution)/shard_map/all_gather | solution.py:60
  15.0 285.5 %all-gather.17.cloned.1.call-start = ((), (), s32[]{:S(2)}) async-start(), calls=%async_computation.1 | async-start | bytes 2293760 | tf_op jit(solution)/shard_map/all_gather | solution.py:41
  115.1 80.8 %copy-start.1 = (bf16[224,4096]{1,0:T(8,128)(2,1)S(1)}, bf16[224,4096]{1,0:T(8,128)(2,1)}, u32[]{:S(2)}) copy-start(bf16[224,4096]{1,0:T(8,128)(2,1)} %all-gather.15.cloned.1.call-done) | copy-start | bytes 5505028
  119.2 81.4 %copy-start.8 = (f32[2,512]{1,0:T(2,128)S(1)}, f32[2,512]{1,0:T(2,128)}, u32[]{:S(2)}) copy-start(f32[2,512]{1,0:T(2,128)} %param.14) | copy-start | bytes 12292
  199.3 2.9 collective-permute-start
  202.2 74.4 %copy-start.3 = (bf16[224,1024]{1,0:T(8,128)(2,1)S(1)}, bf16[224,1024]{1,0:T(8,128)(2,1)}, u32[]{:S(2)}) copy-start(bf16[224,1024]{1,0:T(8,128)(2,1)} %param.8) | copy-start | bytes 1376260
  280.7 101.9 %all-gather.27.cloned.1.call-start = ((), (), s32[]{:S(2)}) async-start(), calls=%async_computation.6 | async-start | bytes 5242880 | tf_op jit(solution)/shard_map/all_gather | solution.py:44
  281.3 182.2 %all-gather.25.cloned.1.call-start = ((), (), s32[]{:S(2)}) async-start(), calls=%async_computation.5 | async-start | bytes 5242880 | tf_op jit(solution)/shard_map/all_gather | solution.py:43
  282.1 262.3 %all-gather.29.cloned.1.call-start = ((), (), s32[]{:S(2)}) async-start(), calls=%async_computation.7 | async-start | bytes 5242880 | tf_op jit(solution)/shard_map/all_gather | solution.py:60
  382.7 80.8 %copy-start.2 = (bf16[224,4096]{1,0:T(8,128)(2,1)S(1)}, bf16[224,4096]{1,0:T(8,128)(2,1)}, u32[]{:S(2)}) copy-start(bf16[224,4096]{1,0:T(8,128)(2,1)} %all-gather.17.cloned.1.call-done) | copy-start | bytes 5505028
  466.9 2.9 collective-permute-start.1
  469.8 74.5 %copy-start.4 = (bf16[224,1024]{1,0:T(8,128)(2,1)S(1)}, bf16[224,1024]{1,0:T(8,128)(2,1)}, u32[]{:S(2)}) copy-start(bf16[224,1024]{1,0:T(8,128)(2,1)} %fusion.27) | copy-start | bytes 1376260
Sparse Core Ops, SparseCore 0:
  8.9 23.8 all-gather.14
  34.3 80.7 all-gather.20
  116.7 79.2 all-gather.18
  197.3 79.2 all-gather.22
  280.8 19.5 all-gather.16
  301.9 80.7 all-gather.26
  384.2 79.2 all-gather.24
  465.1 79.2 all-gather.28
where the time goes:
time: 556 us; the launch traced here: 555 us
  waiting for transfers between devices  468 us (84%)
  blocking collectives  30.7 us (6%)
  matrix products  23.1 us (4%)
  between operations  13.7 us (2%)
  other arithmetic  9.31 us (2%)
  local copies, waits for them, and re-layouts  7.75 us (1%)
    all_gather x2, waiting for transfers between devices, shards(): lax.all_gather(w_gate[layer], 'sp', axis=0, tiled=True)  161 us
    all_gather x2, waiting for transfers between devices, shards(): lax.all_gather(w_value[layer], 'sp', axis=0, tiled=True)  153 us
    all_gather x2, waiting for transfers between devices, shards(): lax.all_gather(w_out[layer], 'sp', axis=0, tiled=True)  113 us
    all_gather x2, waiting for transfers between devices, shards(): whole_rows = lax.all_gather(current, 'tp', axis=1, tiled=True)  35.2 us
    all_gather x2, blocking collectives, shards(): act_all = lax.all_gather(act_t, 'tp', axis=0, tiled=True)  18.2 us
    dot_general x4, matrix products, project_in(): lax.dot_general(weight, columns, (((0,), (1,)), ((), ())), preferred_elem...  14.9 us
    psum x2, blocking collectives, shards(): lax.psum((jnp.sum(conv, axis=0), jnp.sum(conv * conv, axis=0)), 'tp')  12.5 us
  transfers between devices with their start and end apart: 10, of which 10 were waited for; matrix products, arithmetic and copies ran while one was open for 6% of the time, Pallas kernels for 0%

commit v1 on v0

--- a/solution.py
+++ b/solution.py
@@ -38,7 +38,18 @@
     current = tokens
     for layer in range(layers):
         gain = rms_gain[layer]
-        whole_rows = lax.all_gather(current, "tp", axis=1, tiled=True)
+        wide_n = lax.psum(1, "tp")
+        bank = [current]
+        j = 0
+        while j < wide_n - 1:
+            current_arr = lax.ppermute(
+                bank[-1], "tp", [(d, (d + 1) % wide_n) for d in range(wide_n)]
+            )
+            bank.append(current_arr)
+            j = j + 1
+        block_last = jnp.concatenate(bank[::-1], axis=1)
+        known = lax.axis_index("tp")
+        whole_rows = jnp.roll(block_last, (known + 1) * current.shape[1], axis=1)
         normed = norm_rows(whole_rows.astype(jnp.float32), gain)
         value_t = project_in(lax.all_gather(w_value[layer], "sp", axis=0, tiled=True), normed)
         gate_t = project_in(lax.all_gather(w_gate[layer], "sp", axis=0, tiled=True), normed)

time: 556 us -> 508 us (0.914)
  waiting for transfers between devices: 468 us -> 412 us
  other arithmetic: 9.31 us -> 17.9 us
    all_gather x2, waiting for transfers between devices: 161 us -> 94.1 us  [shards(): lax.all_gather(w_gate[layer], 'sp', axis=0, tiled=True)]
    ppermute x0 -> x6, waiting for transfers between devices: none -> 47.5 us  [shards(): lax.ppermute(bank[-1], 'tp', [(d, (d + 1) % wide_n) for d in range(wide_n)])]
    all_gather x2 -> x0, waiting for transfers between devices: 35.2 us -> none  [shards(): whole_rows = lax.all_gather(current, 'tp', axis=1, tiled=True)]
    reduce_sum x2, other arithmetic: 3.88 us -> 12.5 us  [norm_rows(): jnp.mean(wide * wide, axis=1, keepdims=True) + 1e-06]
  transfers between devices with their start and end apart: 10 -> 14, of which waited for: 10 -> 14; matrix products, arithmetic and copies ran while one was open for 6% -> 8% of each run, Pallas kernels for 0% -> 0%
where the time goes in v1:
time: 508 us
  waiting for transfers between devices  412 us (81%)
  blocking collectives  30.7 us (6%)
  matrix products  21.7 us (4%)
  other arithmetic  17.9 us (4%)
  between operations  13.8 us (3%)
  local copies, waits for them, and re-layouts  8.1 us (2%)
    all_gather x2, waiting for transfers between devices, shards(): lax.all_gather(w_value[layer], 'sp', axis=0, tiled=True)  154 us
    all_gather x2, waiting for transfers between devices, shards(): lax.all_gather(w_out[layer], 'sp', axis=0, tiled=True)  113 us
    all_gather x2, waiting for transfers between devices, shards(): lax.all_gather(w_gate[layer], 'sp', axis=0, tiled=True)  94.1 us
    ppermute x6, waiting for transfers between devices, shards(): lax.ppermute(bank[-1], 'tp', [(d, (d + 1) % wide_n) for d in range(wide_n)])  47.5 us
    all_gather x2, blocking collectives, shards(): act_all = lax.all_gather(act_t, 'tp', axis=0, tiled=True)  18.2 us
    dot_general x4, matrix products, project_in(): lax.dot_general(weight, columns, (((0,), (1,)), ((), ())), preferred_elem...  14.4 us
    psum x2, blocking collectives, shards(): lax.psum((jnp.sum(conv, axis=0), jnp.sum(conv * conv, axis=0)), 'tp')  12.5 us
    reduce_sum x2, other arithmetic, norm_rows(): jnp.mean(wide * wide, axis=1, keepdims=True) + 1e-06  12.5 us
  transfers between devices with their start and end apart: 14, of which 14 were waited for; matrix products, arithmetic and copies ran while one was open for 8% of the time, Pallas kernels for 0%

profile of v1, /device:TPU:0, one launch (start us, length us, event | category | flops | bytes accessed | tf_op | source)
XLA Modules:
  0.0 508.0 jit_solution(1724059352905296232)
XLA Ops:
  16.4 8.1 %collective-permute-done = bf16[224,1024]{1,0:T(8,128)(2,1)S(1)} collective-permute-done((bf16[224,1024]{1,0:T(8,128)(2,1)S(1)}, bf16[224,1024]{1,0:T(8,128)(2,1)S(1)}, u32[]{:S(2)}, u32[]{:S(2)}) %collective-permute-start) | collective-permute-done | bytes 458784 | tf_op jit(solution)/shard_map/ppermute | solution.py:45
  24.6 7.8 %collective-permute-done.1 = bf16[224,1024]{1,0:T(8,128)(2,1)S(1)} collective-permute-done((bf16[224,1024]{1,0:T(8,128)(2,1)S(1)}, bf16[224,1024]{1,0:T(8,128)(2,1)S(1)}, u32[]{:S(2)}, u32[]{:S(2)}) %collective-permute-start.1) | collective-permute-done | bytes 458784 | tf_op jit(solution)/shard_map/ppermute | solution.py:45
  32.5 7.9 %collective-permute-done.2 = bf16[224,1024]{1,0:T(8,128)(2,1)} collective-permute-done((bf16[224,1024]{1,0:T(8,128)(2,1)S(1)}, bf16[224,1024]{1,0:T(8,128)(2,1)}, u32[]{:S(2)}, u32[]{:S(2)}) %collective-permute-start.2) | collective-permute-done | bytes 458784 | tf_op jit(solution)/shard_map/ppermute | solution.py:45
  40.4 6.4 %fusion.12 = (f32[224]{0:T(256)S(1)}, bf16[224,4096]{1,0:T(8,128)(2,1)S(1)}) fusion(s32[]{:T(128)S(6)} %select_n.13, bf16[224,1024]{1,0:T(8,128)(2,1)S(1)} %copy-done.1, bf16[224,1024]{1,0:T(8,128)(2,1)S(1)} %collective-permute-done, bf16[224,1024]{1,0:T(8,128)(2,1)S(1)} %collective-permute-done.1, bf16[224,1024]{1,0:T(8,128)(2,1)} %collective-permute-done.2), kind=kLoop, calls=%fused_computation.16 | loop fusion | flops 17432352 | bytes 3670916 | tf_op jit(solution)/shard_map/reduce_sum | solution.py:28
  46.9 46.5 %all-gather.15.cloned.1.call-done = bf16[1,4096,512]{2,1,0:T(8,128)(2,1)} async-done(((bf16[1,1024,512]{2,1,0:T(8,128)(2,1)}), bf16[1,4096,512]{2,1,0:T(8,128)(2,1)}) %all-gather.15.cloned.1.call-update) | async-done | bytes 4194320 | tf_op jit(solution)/shard_map/all_gather | solution.py:55
  93.4 3.4 fusion.71
  96.9 77.4 %all-gather.13.cloned.1.call-done = bf16[1,4096,512]{2,1,0:T(8,128)(2,1)} async-done(((bf16[1,1024,512]{2,1,0:T(8,128)(2,1)}), bf16[1,4096,512]{2,1,0:T(8,128)(2,1)}) %all-gather.13.cloned.1.call-update) | async-done | bytes 4194320 | tf_op jit(solution)/shard_map/all_gather | solution.py:54
  174.2 3.3 fusion.80
  183.0 6.3 %all-reduce.1 = (f32[224]{0:T(256)S(1)}, f32[224]{0:T(256)S(1)}) all-reduce(f32[224]{0:T(256)S(1)} %get-tuple-element.9, f32[224]{0:T(256)S(1)} %get-tuple-element.8), channel_id=1, replica_groups=mesh['grp'=2,'sp'=4,'tp'=4] {'tp'}, use_global_device_ids=true, to_apply=%region_4.6 | all-reduce | flops 448 | bytes 3584 | tf_op jit(solution)/shard_map/psum | solution.py:63
  189.5 9.1 %all_gather.26 = bf16[2048,224]{0,1:T(8,128)(2,1)S(1)} all-gather(bf16[512,224]{0,1:T(8,128)(2,1)S(1)} %multiply_convert_fusion.1), channel_id=1, replica_groups=mesh['grp'=2,'sp'=4,'tp'=4] {'tp'}, dimensions={0}, use_global_device_ids=true | all-gather | bytes 1146880 | tf_op jit(solution)/shard_map/all_gather | solution.py:70
  198.6 56.5 %all-gather.17.cloned.1.call-done = bf16[1,2048,1024]{2,1,0:T(8,128)(2,1)} async-done(((bf16[1,512,1024]{2,1,0:T(8,128)(2,1)}), bf16[1,2048,1024]{2,1,0:T(8,128)(2,1)}) %all-gather.17.cloned.1.call-update) | async-done | bytes 4194320 | tf_op jit(solution)/shard_map/all_gather | solution.py:71
  255.1 3.3 fusion.41
  258.5 7.9 %collective-permute-done.4 = bf16[224,1024]{1,0:T(8,128)(2,1)S(1)} collective-permute-done((bf16[224,1024]{1,0:T(8,128)(2,1)S(1)}, bf16[224,1024]{1,0:T(8,128)(2,1)S(1)}, u32[]{:S(2)}, u32[]{:S(2)}) %collective-permute-start.4) | collective-permute-done | bytes 458784 | tf_op jit(solution)/shard_map/ppermute | solution.py:45
  266.3 7.9 %collective-permute-done.5 = bf16[224,1024]{1,0:T(8,128)(2,1)S(1)} collective-permute-done((bf16[224,1024]{1,0:T(8,128)(2,1)S(1)}, bf16[224,1024]{1,0:T(8,128)(2,1)S(1)}, u32[]{:S(2)}, u32[]{:S(2)}) %collective-permute-start.5) | collective-permute-done | bytes 458784 | tf_op jit(solution)/shard_map/ppermute | solution.py:45
  274.3 7.9 %collective-permute-done.6 = bf16[224,1024]{1,0:T(8,128)(2,1)S(1)} collective-permute-done((bf16[224,1024]{1,0:T(8,128)(2,1)S(1)}, bf16[224,1024]{1,0:T(8,128)(2,1)S(1)}, u32[]{:S(2)}, u32[]{:S(2)}) %collective-permute-start.6) | collective-permute-done | bytes 458784 | tf_op jit(solution)/shard_map/ppermute | solution.py:45
  282.2 6.0 %fusion.15 = (f32[224]{0:T(256)S(1)}, bf16[224,4096]{1,0:T(8,128)(2,1)S(1)}) fusion(s32[]{:T(128)S(6)} %select_n.13, bf16[224,1024]{1,0:T(8,128)(2,1)S(1)} %fusion.41, bf16[224,1024]{1,0:T(8,128)(2,1)S(1)} %collective-permute-done.4, bf16[224,1024]{1,0:T(8,128)(2,1)S(1)} %collective-permute-done.5, bf16[224,1024]{1,0:T(8,128)(2,1)S(1)} %collective-permute-done.6), kind=kLoop, calls=%fused_computation.19 | loop fusion | flops 17432352 | bytes 3670916 | tf_op jit(solution)/shard_map/reduce_sum | solution.py:28
  288.2 47.6 %all-gather.21.cloned.1.call-done = bf16[1,4096,512]{2,1,0:T(8,128)(2,1)} async-done(((bf16[1,1024,512]{2,1,0:T(8,128)(2,1)}), bf16[1,4096,512]{2,1,0:T(8,128)(2,1)}) %all-gather.21.cloned.1.call-update) | async-done | bytes 4194320 | tf_op jit(solution)/shard_map/all_gather | solution.py:55
  335.8 4.2 fusion.65
  339.9 76.5 %all-gather.19.cloned.1.call-done = bf16[1,4096,512]{2,1,0:T(8,128)(2,1)} async-done(((bf16[1,1024,512]{2,1,0:T(8,128)(2,1)}), bf16[1,4096,512]{2,1,0:T(8,128)(2,1)}) %all-gather.19.cloned.1.call-update) | async-done | bytes 4194320 | tf_op jit(solution)/shard_map/all_gather | solution.py:54
  416.4 3.4 fusion.83
  425.2 6.3 %all-reduce = (f32[224]{0:T(256)S(1)}, f32[224]{0:T(256)S(1)}) all-reduce(f32[224]{0:T(256)S(1)} %get-tuple-element.7, f32[224]{0:T(256)S(1)} %get-tuple-element.6), channel_id=1, replica_groups=mesh['grp'=2,'sp'=4,'tp'=4] {'tp'}, use_global_device_ids=true, to_apply=%region_9.11 | all-reduce | flops 448 | bytes 3584 | tf_op jit(solution)/shard_map/psum | solution.py:63
  431.8 9.1 %all_gather.30 = bf16[2048,224]{0,1:T(8,128)(2,1)S(1)} all-gather(bf16[512,224]{0,1:T(8,128)(2,1)S(1)} %multiply_convert_fusion), channel_id=1, replica_groups=mesh['grp'=2,'sp'=4,'tp'=4] {'tp'}, dimensions={0}, use_global_device_ids=true | all-gather | bytes 1146880 | tf_op jit(solution)/shard_map/all_gather | solution.py:70
  440.9 56.3 %all-gather.23.cloned.1.call-done = bf16[1,2048,1024]{2,1,0:T(8,128)(2,1)} async-done(((bf16[1,512,1024]{2,1,0:T(8,128)(2,1)}), bf16[1,2048,1024]{2,1,0:T(8,128)(2,1)}) %all-gather.23.cloned.1.call-update) | async-done | bytes 4194320 | tf_op jit(solution)/shard_map/all_gather | solution.py:71
  497.1 4.1 fusion.38
  (56 shorter events, 21.1 us)
Async XLA Ops:
  6.5 3.3 copy-start
  6.5 86.9 %all-gather.15.cloned.1.call-start = ((), (), s32[]{:S(2)}) async-start(), calls=%async_computation.1 | async-start | bytes 5242880 | tf_op jit(solution)/shard_map/all_gather | solution.py:55
  9.8 164.4 %all-gather.13.cloned.1.call-start = ((), (), s32[]{:S(2)}) async-start(), calls=%async_computation | async-start | bytes 5242880 | tf_op jit(solution)/shard_map/all_gather | solution.py:54
  11.4 4.4 copy-start.1
  11.4 13.1 %copy-start.3 = (f32[2,4096]{1,0:T(2,128)S(1)}, f32[2,4096]{1,0:T(2,128)}, u32[]{:S(2)}) copy-start(f32[2,4096]{1,0:T(2,128)} %param.11) | copy-start | bytes 98308
  11.4 13.1 %copy-start.2 = (f32[2,31,512]{2,0,1:T(2,128)S(1)}, f32[2,31,512]{2,0,1:T(2,128)}, u32[]{:S(2)}) copy-start(f32[2,31,512]{2,0,1:T(2,128)} %param.14) | copy-start | bytes 380932
  11.4 21.0 %copy-start.4 = (f32[2,512]{1,0:T(2,128)S(1)}, f32[2,512]{1,0:T(2,128)}, u32[]{:S(2)}) copy-start(f32[2,512]{1,0:T(2,128)} %param.15) | copy-start | bytes 12292
  11.5 243.6 %all-gather.17.cloned.1.call-start = ((), (), s32[]{:S(2)}) async-start(), calls=%async_computation.2 | async-start | bytes 5242880 | tf_op jit(solution)/shard_map/all_gather | solution.py:71
  14.6 321.1 %all-gather.21.cloned.1.call-start = ((), (), s32[]{:S(2)}) async-start(), calls=%async_computation.4 | async-start | bytes 5242880 | tf_op jit(solution)/shard_map/all_gather | solution.py:55
  15.2 401.2 %all-gather.19.cloned.1.call-start = ((), (), s32[]{:S(2)}) async-start(), calls=%async_computation.3 | async-start | bytes 5242880 | tf_op jit(solution)/shard_map/all_gather | solution.py:54
  15.8 481.3 %all-gather.23.cloned.1.call-start = ((), (), s32[]{:S(2)}) async-start(), calls=%async_computation.5 | async-start | bytes 5242880 | tf_op jit(solution)/shard_map/all_gather | solution.py:71
  15.9 8.7 %collective-permute-start = (bf16[224,1024]{1,0:T(8,128)(2,1)S(1)}, bf16[224,1024]{1,0:T(8,128)(2,1)S(1)}, u32[]{:S(2)}, u32[]{:S(2)}) collective-permute-start(bf16[224,1024]{1,0:T(8,128)(2,1)S(1)} %copy-done.1), channel_id=1, source_target_pairs={{0,1},{1,2},{2,3},{3,0},{4,5},{5,6},{6,7},{7,4},{8,9},{9,10},{10,1... | collective-permute-start | bytes 1376264 | tf_op jit(solution)/shard_map/ppermute | solution.py:45
  24.5 7.9 %collective-permute-start.1 = (bf16[224,1024]{1,0:T(8,128)(2,1)S(1)}, bf16[224,1024]{1,0:T(8,128)(2,1)S(1)}, u32[]{:S(2)}, u32[]{:S(2)}) collective-permute-start(bf16[224,1024]{1,0:T(8,128)(2,1)S(1)} %collective-permute-done), channel_id=1, source_target_pairs={{0,1},{1,2},{2,3},{3,0},{4,5},{5,6},{6,7},{7,4},{8,9},{9,10},{10,1... | collective-permute-start | bytes 1376264 | tf_op jit(solution)/shard_map/ppermute | solution.py:45
  32.4 8.0 %collective-permute-start.2 = (bf16[224,1024]{1,0:T(8,128)(2,1)S(1)}, bf16[224,1024]{1,0:T(8,128)(2,1)}, u32[]{:S(2)}, u32[]{:S(2)}) collective-permute-start(bf16[224,1024]{1,0:T(8,128)(2,1)S(1)} %collective-permute-done.1), channel_id=1, source_target_pairs={{0,1},{1,2},{2,3},{3,0},{4,5},{5,6},{6,7},{7,4},{8,9},{9,10},{10,1... | collective-permute-start | bytes 1376264 | tf_op jit(solution)/shard_map/ppermute | solution.py:45
  96.8 82.1 %copy-start.5 = (f32[2,512]{1,0:T(2,128)S(1)}, f32[2,512]{1,0:T(2,128)}, u32[]{:S(2)}) copy-start(f32[2,512]{1,0:T(2,128)} %param.16) | copy-start | bytes 12292
  177.6 2.9 collective-permute-start.3
  258.4 8.0 %collective-permute-start.4 = (bf16[224,1024]{1,0:T(8,128)(2,1)S(1)}, bf16[224,1024]{1,0:T(8,128)(2,1)S(1)}, u32[]{:S(2)}, u32[]{:S(2)}) collective-permute-start(bf16[224,1024]{1,0:T(8,128)(2,1)S(1)} %fusion.41), channel_id=1, source_target_pairs={{0,1},{1,2},{2,3},{3,0},{4,5},{5,6},{6,7},{7,4},{8,9},{9,10},{10,1... | collective-permute-start | bytes 1376264 | tf_op jit(solution)/shard_map/ppermute | solution.py:45
  266.3 7.9 %collective-permute-start.5 = (bf16[224,1024]{1,0:T(8,128)(2,1)S(1)}, bf16[224,1024]{1,0:T(8,128)(2,1)S(1)}, u32[]{:S(2)}, u32[]{:S(2)}) collective-permute-start(bf16[224,1024]{1,0:T(8,128)(2,1)S(1)} %collective-permute-done.4), channel_id=1, source_target_pairs={{0,1},{1,2},{2,3},{3,0},{4,5},{5,6},{6,7},{7,4},{8,9},{9,10},{10,1... | collective-permute-start | bytes 1376264 | tf_op jit(solution)/shard_map/ppermute | solution.py:45
  274.3 7.9 %collective-permute-start.6 = (bf16[224,1024]{1,0:T(8,128)(2,1)S(1)}, bf16[224,1024]{1,0:T(8,128)(2,1)S(1)}, u32[]{:S(2)}, u32[]{:S(2)}) collective-permute-start(bf16[224,1024]{1,0:T(8,128)(2,1)S(1)} %collective-permute-done.5), channel_id=1, source_target_pairs={{0,1},{1,2},{2,3},{3,0},{4,5},{5,6},{6,7},{7,4},{8,9},{9,10},{10,1... | collective-permute-start | bytes 1376264 | tf_op jit(solution)/shard_map/ppermute | solution.py:45
  419.9 2.9 collective-permute-start.7
Sparse Core Ops, SparseCore 0:
  9.9 83.4 all-gather.14
  95.0 79.2 all-gather.12
  175.8 79.2 all-gather.16
  256.5 79.2 all-gather.20
  337.2 79.2 all-gather.18
  417.9 79.2 all-gather.22
